TPU v7x, 128 devices: a whole 4x4x4 slice. The times are simulated.
128 devices in a mesh: sp: 32 (over z, y, core), tp: 4 (over x).
Axes of the slice: x: 4, y: 4, z: 4, core: 2. Of those that a mesh axis runs over, the one named last changes fastest.
Arguments:
- tokens: bfloat16 [16384, 2048], P(('sp', 'tp')), may hold values from -6 to 6
- norm_gain: float32 [2048], replicated, may hold values from 0.1 to 1.9
- query_weight: bfloat16 [2048, 2048], P('sp', 'tp'), may hold values from -0.125 to 0.125
- key_weight: bfloat16 [2048, 2048], P('sp', 'tp'), may hold values from -0.125 to 0.125
- value_weight: bfloat16 [2048, 4096], P('sp', 'tp'), may hold values from -0.125 to 0.125
- retain_gate: bfloat16 [2048, 4096], P('sp', 'tp'), may hold values from -0.125 to 0.125
- unit_value: bfloat16 [2048, 2048], P('sp', 'tp'), may hold values from -0.125 to 0.125
- unit_gate: bfloat16 [2048, 2048], P('sp', 'tp'), may hold values from -0.125 to 0.125
- convolve_gate: bfloat16 [2048, 2048], P('sp', 'tp'), may hold values from -0.125 to 0.125
- filter_taps: float32 [31, 2048], replicated, may hold values from -1 to 1
- layer_gain: float32 [2048], replicated, may hold values from 0.1 to 1.9
- layer_shift: float32 [2048], replicated, may hold values from -3 to 3
- retain_output: bfloat16 [2048, 4096], P('sp', 'tp'), may hold values from -0.09375 to 0.09375
- convolve_output: bfloat16 [2048, 2048], P('sp', 'tp'), may hold values from -0.125 to 0.125
Outputs:
- mixed: bfloat16 [16384, 2048], P(('sp', 'tp'))
All inputs are finite; a program needn't handle non-finite values.
Results may differ from a plain program's by a relative error of at most 0.018.
Values may be sent and summed in bfloat16 or wider, within the bound.
A program may use at most 128 MiB of HBM per device.

v0:
```python
import jax
import jax.numpy as jnp
from jax import lax
from jax.sharding import Mesh
from jax.sharding import PartitionSpec as P

KEY = 256
VAL = 512
GROUP = 512
KW = 31
SP = ("sp_0", "sp_1", "sp_2")
SP_TP = ("sp_0", "sp_1", "sp_2", "tp")


rms_eps = 1e-06
group_eps = 1.0
layer_eps = 0.001
rope_base = 10000.0


def in_one_piece(arrays, axis, dim, along):
    ends, at = ([], 0)
    for a in arrays[:-1]:
        at += a.shape[along]
        ends.append(at)
    both = jnp.concatenate(arrays, axis=along)
    return tuple(jnp.split(lax.all_gather(both, axis, axis=dim, tiled=True), ends, axis=along))


def copy_for_each(x, axis):
    copies = jnp.broadcast_to(x, (lax.axis_size(axis), *x.shape))
    return lax.all_to_all(copies, axis, split_axis=0, concat_axis=0, tiled=True)


def in_order(parts, dim):
    parts = jnp.moveaxis(parts, 0, dim)
    lengths = parts.shape
    return parts.reshape(*lengths[:dim], lengths[dim] * lengths[dim + 1], *lengths[dim + 2 :])


def gather_directly(x, axis, dim):
    parts = copy_for_each(x, axis)
    return in_order(parts, dim)


def filled_with(x, identity):
    return jax.tree.map(
        lambda a, e: jnp.broadcast_to(jnp.asarray(e, a.dtype), a.shape), x, identity
    )


def entering(x, axes, combine, identity):
    before = start = filled_with(x, identity)
    total = x
    for axis in reversed(axes):
        length, place = (lax.axis_size(axis), lax.axis_index(axis))
        pieces = jax.tree.map(lambda part: lax.all_gather(part, axis), total)
        inside, total = (start, start)
        for k in range(length):
            passed = k < place
            total = combine(total, jax.tree.map(lambda part: part[k], pieces))
            inside = jax.tree.map(lambda new, old: jnp.where(passed, new, old), total, inside)
        before = combine(inside, before)
    return before


def from_behind(x, axis, by):
    length = lax.axis_size(axis)
    pairs = [(i, i + by) for i in range(length) if 0 <= i + by < length]
    return lax.ppermute(x, axis, pairs)


def rms_normalize(tokens, norm_gain):
    widened = tokens.astype(jnp.float32)
    scaled = widened * lax.rsqrt(jnp.mean(widened * widened, axis=-1, keepdims=True) + rms_eps)
    return (scaled * norm_gain).astype(jnp.bfloat16)


def rotate(vectors, positions):
    half_width = vectors.shape[-1] // 2
    frequency = rope_base ** (-jnp.arange(half_width, dtype=jnp.float32) / half_width)
    angles = positions.astype(jnp.float32)[:, None] * frequency
    cosine = jnp.cos(angles)[:, None, :]
    sine_part = jnp.sin(angles)[:, None, :]
    front_half = vectors[..., :half_width]
    back_half = vectors[..., half_width:]
    return jnp.concatenate(
        [front_half * cosine - back_half * sine_part, front_half * sine_part + back_half * cosine],
        axis=-1,
    )


def prepare(queries, key_rows, values, positions):
    row_count = queries.shape[0]
    rotated_query = rotate(
        queries.astype(jnp.float32).reshape(row_count, -1, KEY), positions
    ).astype(jnp.bfloat16)
    rotated_keys = (
        rotate(key_rows.astype(jnp.float32).reshape(row_count, -1, KEY), positions) * KEY ** (-0.5)
    ).astype(jnp.bfloat16)
    value_heads = values.reshape(row_count, -1, VAL)
    return (rotated_query, rotated_keys, value_heads)


def decay_logs(first_head, head_total, all_heads, seq_length):
    ratio = (first_head + jnp.arange(head_total)).astype(jnp.float32) / (all_heads - 1)
    return (jnp.log(0.05) + ratio * jnp.log(18.0)) / seq_length


def local_parts(queries, key_rows, values, log_decay):
    row_count = queries.shape[0]
    indices = jnp.arange(row_count, dtype=jnp.float32)
    offsets = indices[:, None] - indices[None, :]
    causal = offsets >= 0
    weight = jnp.where(
        causal[None], jnp.exp(log_decay[:, None, None] * jnp.where(causal, offsets, 0.0)[None]), 0.0
    )
    scores = (
        jnp.einsum("ihd,jhd->hij", queries, key_rows, preferred_element_type=jnp.float32) * weight
    ).astype(jnp.bfloat16)
    within = jnp.einsum("hij,jhe->ihe", scores, values, preferred_element_type=jnp.float32)
    trailing = jnp.exp(log_decay[None, :] * (row_count - 1.0 - indices)[:, None])
    weighted = (key_rows.astype(jnp.float32) * trailing[:, :, None]).astype(jnp.bfloat16)
    contribution = jnp.einsum("jhd,jhe->hde", weighted, values, preferred_element_type=jnp.float32)
    return (within, contribution)


def cross_part(queries, carry_state, log_decay):
    row_count = queries.shape[0]
    indices = jnp.arange(row_count, dtype=jnp.float32)
    leading = jnp.exp(log_decay[None, :] * (indices + 1.0)[:, None])
    return (
        jnp.einsum("ihd,hde->ihe", queries.astype(jnp.float32), carry_state) * leading[:, :, None]
    )


def retain_finish(raw, switch):
    average = jnp.mean(raw, axis=-1, keepdims=True)
    spread = jnp.mean(jnp.square(raw - average), axis=-1, keepdims=True)
    normalized = ((raw - average) * lax.rsqrt(spread + group_eps)).reshape(raw.shape[0], -1)
    return (normalized * jax.nn.silu(switch.astype(jnp.float32))).astype(jnp.bfloat16)


def convolve_branch(gated_input, before, tap_slice, gain_slice, shift_slice, switch):
    padded = jnp.concatenate([before, gated_input], axis=0)
    row_count = gated_input.shape[0]
    summed = jnp.zeros(gated_input.shape, jnp.float32)
    for tap_index in range(tap_slice.shape[0]):
        summed = (
            summed
            + padded[tap_index : tap_index + row_count].astype(jnp.float32) * tap_slice[tap_index]
        )
    grouped = summed.reshape(row_count, -1, GROUP)
    average = jnp.mean(grouped, axis=-1, keepdims=True)
    spread = jnp.mean(jnp.square(grouped - average), axis=-1, keepdims=True)
    normalized = ((grouped - average) * lax.rsqrt(spread + layer_eps)).reshape(row_count, -1)
    normalized = normalized * gain_slice + shift_slice
    return (jax.nn.silu(normalized) * jax.nn.silu(switch.astype(jnp.float32))).astype(jnp.bfloat16)


def contract(hidden, matrix):
    return lax.dot_general(
        hidden, matrix, (((1,), (1,)), ((), ())), preferred_element_type=jnp.float32
    )


def join_states(earlier, later):
    return (earlier[0] * later[0], later[0][:, None, None] * earlier[1] + later[1])


def local(
    tokens,
    norm_gain,
    query_weight,
    key_weight,
    value_weight,
    retain_gate,
    unit_value,
    unit_gate,
    convolve_gate,
    filter_taps,
    layer_gain,
    layer_shift,
    retain_output,
    convolve_output,
):
    head_groups = lax.axis_size("tp")
    chain_length = lax.axis_size(SP)
    head_rank = lax.axis_index("tp")
    chain_rank = lax.axis_index(SP)
    normed = rms_normalize(tokens, norm_gain)
    gathered = in_one_piece(
        (
            query_weight,
            key_weight,
            value_weight,
            retain_gate,
            unit_value,
            unit_gate,
            convolve_gate,
            retain_output,
            convolve_output,
        ),
        SP,
        0,
        1,
    )
    in_weights = gathered[:7]
    retain_full = gathered[7]
    convolve_full = gathered[8]

    def project(row_piece):
        return jnp.concatenate(
            [
                jnp.dot(row_piece, matrix, preferred_element_type=jnp.float32).astype(jnp.bfloat16)
                for matrix in in_weights
            ],
            axis=1,
        )

    projected = project(gather_directly(normed, "tp", 0))
    row_count = projected.shape[0]
    bounds = [0]
    for matrix in in_weights:
        bounds.append(bounds[-1] + matrix.shape[1])
    pieces = [projected[:, bounds[column] : bounds[column + 1]] for column in range(7)]
    queries, key_rows, values, retain_switch, glu_value, glu_switch, convolve_switch = pieces
    local_heads = queries.shape[1] // KEY
    positions = chain_rank * row_count + jnp.arange(row_count, dtype=jnp.int32)
    rotated_query, rotated_keys, value_heads = prepare(queries, key_rows, values, positions)
    log_decay = decay_logs(
        head_rank * local_heads, local_heads, local_heads * head_groups, row_count * chain_length
    )
    within, contribution = local_parts(rotated_query, rotated_keys, value_heads, log_decay)
    totals = jnp.exp(log_decay * row_count)
    gated_input = (
        glu_value.astype(jnp.float32) * jax.nn.sigmoid(glu_switch.astype(jnp.float32))
    ).astype(jnp.bfloat16)
    channels = gated_input.shape[1]
    before = from_behind(gated_input[row_count - (KW - 1) :], SP, 1)
    prefix = entering(
        (totals, contribution),
        SP,
        join_states,
        (jnp.ones_like(totals), jnp.zeros_like(contribution)),
    )
    incoming = prefix[1]
    raw = within + cross_part(rotated_query, incoming, log_decay)
    retain_hidden = retain_finish(raw, retain_switch)
    tap_slice = lax.dynamic_slice_in_dim(filter_taps, head_rank * channels, channels, 1)
    gain_slice = lax.dynamic_slice_in_dim(layer_gain, head_rank * channels, channels, 0)
    shift_slice = lax.dynamic_slice_in_dim(layer_shift, head_rank * channels, channels, 0)
    convolve_hidden = convolve_branch(
        gated_input, before, tap_slice, gain_slice, shift_slice, convolve_switch
    )
    return lax.psum_scatter(
        (contract(retain_hidden, retain_full) + contract(convolve_hidden, convolve_full)).astype(
            jnp.bfloat16
        ),
        "tp",
        scatter_dimension=0,
        tiled=True,
    )


def solution(mesh):
    finer = Mesh(mesh.devices.reshape(4, 4, 2, mesh.shape["tp"]), ("sp_0", "sp_1", "sp_2", "tp"))
    placed = (
        P(SP_TP, None),
        P(),
        P(SP, "tp"),
        P(SP, "tp"),
        P(SP, "tp"),
        P(SP, "tp"),
        P(SP, "tp"),
        P(SP, "tp"),
        P(SP, "tp"),
        P(),
        P(),
        P(),
        P(SP, "tp"),
        P(SP, "tp"),
    )
    return jax.shard_map(
        local, mesh=finer, in_specs=placed, out_specs=P(SP_TP, None), check_vma=False
    )
```

profile of v0, /device:TPU:0, one launch (start us, length us, event | category | flops | bytes accessed | tf_op | source)
XLA Modules:
  0.0 311.4 jit_solution(10433780597011158818)
XLA Ops:
  6.5 0.9 constant_dynamic-update-slice_fusion.8
  7.4 0.8 constant_dynamic-update-slice_fusion.7
  8.3 0.9 constant_dynamic-update-slice_fusion.6
  9.2 0.9 constant_dynamic-update-slice_fusion.5
  10.1 0.8 constant_dynamic-update-slice_fusion.4
  11.0 0.8 constant_dynamic-update-slice_fusion.3
  11.8 0.8 constant_dynamic-update-slice_fusion.2
  12.7 0.9 constant_dynamic-update-slice_fusion.1
  13.6 0.8 constant_dynamic-update-slice_fusion
  14.4 0.9 copy-done.4
  15.3 0.2 fusion.73
  15.5 0.2 fusion.75
  15.7 1.6 broadcast_in_dim.18
  17.4 4.4 %all-to-all-start = ((bf16[4,128,2048]{2,1,0:T(8,128)(2,1)}), bf16[4,128,2048]{2,1,0:T(8,128)(2,1)S(1)}, u32[]{:S(2)}, u32[]{:S(2)}) async-start(bf16[4,128,2048]{2,1,0:T(8,128)(2,1)} %broadcast_in_dim.18), calls=%async_computation | async-start | bytes 4194304 | tf_op jit(solution)/shard_map/all_to_all | solution.py:32
  21.8 0.7 multiply_exponential_fusion
  22.5 1.7 multiply_cosine_fusion
  24.2 23.9 %all-to-all-done = bf16[4,128,2048]{2,1,0:T(8,128)(2,1)S(1)} async-done(((bf16[4,128,2048]{2,1,0:T(8,128)(2,1)}), bf16[4,128,2048]{2,1,0:T(8,128)(2,1)S(1)}, u32[]{:S(2)}, u32[]{:S(2)}) %all-to-all-start) | async-done | bytes 2097184 | tf_op jit(solution)/shard_map/all_to_all | solution.py:32
  48.1 61.9 %all-gather.9.cloned.1.call-done = bf16[2048,6144]{1,0:T(8,128)(2,1)} async-done(((bf16[64,6144]{1,0:T(8,128)(2,1)}), bf16[2048,6144]{1,0:T(8,128)(2,1)}) %all-gather.9.cloned.1.call-update) | async-done | bytes 25165840 | tf_op jit(solution)/shard_map/all_gather | solution.py:27
  110.0 2.9 fusion.30
  112.9 0.1 fusion.215
  113.0 1.0 copy.35
  114.0 1.0 copy.36
  115.1 2.9 fusion.33
  118.0 0.1 fusion.214
  118.1 1.0 copy.37
  119.1 0.2 copy.38
  119.3 2.5 multiply_subtract_fusion
  121.8 4.9 %fusion.23 = bf16[512,1024]{1,0:T(8,128)(2,1)S(1)} fusion(bf16[512,2048]{1,0:T(8,128)(2,1)S(1)} %bitcast.181, bf16[2048,6144]{1,0:T(8,128)(2,1)} %all-gather.9.cloned.1.call-done), kind=kOutput, calls=%fused_computation.59 | convolution fusion | flops 2148007936 | bytes 7340032 | tf_op jit(solution)/shard_map/dot_general | solution.py:215
  126.8 0.9 copy-done.27
  127.7 1.6 fusion.81
  129.4 0.0 all-gather.11.cloned.1.call-start
  129.4 1.8 all-gather.1
  131.2 9.7 %all-gather.2 = f32[4,1,2]{2,1,0:T(1,128)S(1)} all-gather(f32[1,1,2]{2,1,0:T(1,128)S(1)} %get-tuple-element.62), channel_id=1, replica_groups=mesh['sp_0'=4,'sp_1'=4,'sp_2'=2,'tp'=4] {'sp_1'}, dimensions={0}, use_global_device_ids=true | all-gather | bytes 40 | tf_op jit(solution)/shard_map/all_gather | solution.py:57
  140.9 0.6 fusion.198
  141.5 0.5 all-gather.15.cloned.1.call-done
  142.1 2.8 bitcast_add_fusion.4
  144.9 0.0 all-gather.13.cloned.1.call-start
  145.0 49.6 %all-gather.11.cloned.1.call-done = f32[4,2,256,512]{3,2,1,0:T(8,128)} async-done(((f32[1,2,256,512]{3,2,1,0:T(8,128)}), f32[4,2,256,512]{3,2,1,0:T(8,128)}) %all-gather.11.cloned.1.call-update) | async-done | bytes 4194320 | tf_op jit(solution)/shard_map/all_gather | solution.py:57
  194.6 3.8 %multiply_add_fusion.1 = f32[1,2,256,512]{3,2,1,0:T(8,128)} fusion(f32[4,2,256,512]{3,2,1,0:T(8,128)} %all-gather.11.cloned.1.call-done, f32[2]{0:T(128)S(1)} %get-tuple-element.60, f32[2]{0:T(128)S(1)} %get-tuple-element.59, f32[2]{0:T(128)S(1)} %get-tuple-element.58, f32[2]{0:T(128)S(1)} %get-tuple-element.57), kind=kLoop, calls=%fused_computation.132 | loop fusion | flops 1835008 | bytes 5242912 | tf_op jit(solution)/shard_map/add | solution.py:168
  198.4 0.0 all-gather.13.cloned.1.call-update
  198.4 0.0 reduce-scatter.2.cloned.1.call-start
  198.5 9.9 %all-gather.3 = f32[4,1,2]{2,1,0:T(1,128)S(1)} all-gather(f32[1,1,2]{2,1,0:T(1,128)S(1)} %get-tuple-element.56), channel_id=1, replica_groups=mesh['sp_0'=4,'sp_1'=4,'sp_2'=2,'tp'=4] {'sp_0'}, dimensions={0}, use_global_device_ids=true | all-gather | bytes 40 | tf_op jit(solution)/shard_map/all_gather | solution.py:57
  208.4 1.4 dynamic_slice.10
  209.8 1.3 dynamic_slice.11
  211.1 1.2 fusion.216
  212.3 2.0 constant_dynamic-slice_fusion
  214.3 1.0 fusion.122
  215.3 0.2 fusion.121
  215.5 0.6 slice_bitcast_fusion.6
  216.1 3.0 fusion.66
  219.1 2.9 fusion.63
  222.0 0.8 copy-done.5
  222.8 1.5 collective-permute-start
  224.3 4.3 %fusion.29 = f32[2,512,512]{2,1,0:T(8,128)} fusion(f32[512,512]{1,0:T(8,128)S(1)} %fusion.121, f32[2]{0:T(128)} %copy-done.25, pred[512,512]{1,0:T(8,128)(4,1)} %fusion.122, bf16[64,2,8,512]{3,2,1,0:T(8,128)(2,1)} %bitcast.220, bf16[512,2,128]{2,0,1:T(8,128)(2,1)S(1)} %copy-done.8, bf16[512,2,128]{2,0,1:T(8,128)(2,1)} %get-tuple-element.14, ...), kind=kOutput, calls=%fused_computation.61 | convolution fusion | flops 809238528 | bytes 6029320 | tf_op jit(solution)/shard_map/hij,jhe->ihe/dot_general | solution.py:121
  228.7 16.1 %fusion.213 = (f32[512]{0:T(512)S(1)}, f32[512,512]{1,0:T(8,128)S(1)}) fusion(f32[512]{0:T(512)S(1)} %bitcast.200, bf16[512,512]{1,0:T(8,128)(2,1)} %copy-done.5, f32[512]{0:T(512)S(1)} %bitcast.202, bf16[30,512]{1,0:T(8,128)(2,1)S(1)} %collective-permute-done, f32[512]{0:T(512)S(1)} %bitcast.203, f32[512]{0:T(512)S(1)} %bitcast.204, f32[512]{0:T(512)S(1)} %bitcast.205, ...), kind=kLoop, calls=%fused_computation.276 | loop fusion | flops 47971840 | bytes 1669120 | tf_op jit(solution)/shard_map/reduce_sum | solution.py:154
  244.8 0.3 multiply_reduce_fusion.1
  245.0 2.3 all-gather.13.cloned.1.call-done
  247.4 6.0 %fusion.217 = (f32[512,2]{0,1:T(2,128)S(1)}, f32[512,2,512]{0,2,1:T(8,128)S(1)}) fusion(f32[512,2]{0,1:T(2,128)S(1)} %copy-done.10, bf16[512,2,128]{2,0,1:T(8,128)(2,1)S(1)} %copy-done.8, bf16[512,2,128]{2,0,1:T(8,128)(2,1)} %get-tuple-element.14, f32[4,2,256,512]{3,2,1,0:T(8,128)} %all-gather.13.cloned.1.call-done, ...), kind=kOutput, calls=%fused_computation.280 | convolution fusion | flops 279182336 | bytes 15212650 | tf_op jit(solution)/shard_map/ihd,hde->ihe/dot_general | solution.py:133
  253.4 0.3 multiply_reduce_fusion
  253.7 0.3 subtract_multiply_fusion
  253.9 1.8 copy.32
  255.8 11.6 %fusion = f32[512,2048]{1,0:T(8,128)} fusion(bf16[2048,6144]{1,0:T(8,128)(2,1)} %all-gather.9.cloned.1.call-done, f32[512,1024]{1,0:T(8,128)} %copy.32, bf16[512,2048]{1,0:T(8,128)(2,1)} %bitcast.184), kind=kOutput, calls=%fused_computation.29 | convolution fusion | flops 4299161600 | bytes 16777216 | tf_op jit(solution)/shard_map/dot_general | solution.py:162
  267.4 7.5 %add_convert_fusion = bf16[512,2048]{1,0:T(8,128)(2,1)} fusion(f32[512,2048]{1,0:T(8,128)} %fusion, bf16[2048,6144]{1,0:T(8,128)(2,1)} %all-gather.9.cloned.1.call-done, f32[512,512]{1,0:T(8,128)S(1)} %get-tuple-element.6, bf16[512,2048]{1,0:T(8,128)(2,1)S(1)} %bitcast.185, f32[512]{0:T(512)S(1)} %copy-done.24, f32[512]{0:T(512)S(1)} %copy-done.23, ...), kind=kOutput, calls=%fused_computation.35 | convolution fusion | flops 2153775104 | bytes 13639680 | tf_op jit(solution)/shard_map/dot_general | solution.py:162
  274.9 30.0 %reduce-scatter.2.cloned.1.call-done = bf16[128,2048]{1,0:T(8,128)(2,1)} async-done(((bf16[512,2048]{1,0:T(8,128)(2,1)}), bf16[128,2048]{1,0:T(8,128)(2,1)}) %reduce-scatter.2.cloned.1.call-update) | async-done | bytes 524304 | tf_op jit(solution)/shard_map/reduce_scatter | solution.py:256
  (73 shorter events, 0.3 us)
Async XLA Ops:
  6.5 8.8 %copy-start.3 = (bf16[128,2048]{1,0:T(8,128)(2,1)S(1)}, bf16[128,2048]{1,0:T(8,128)(2,1)}, u32[]{:S(2)}) copy-start(bf16[128,2048]{1,0:T(8,128)(2,1)} %param.14) | copy-start | bytes 1572868
  6.5 9.0 %copy-start.9 = (f32[2048]{0:T(1024)S(1)}, f32[2048]{0:T(1024)}, u32[]{:S(2)}) copy-start(f32[2048]{0:T(1024)} %param.15) | copy-start | bytes 24580
  6.5 103.5 %all-gather.9.cloned.1.call-start = ((), (), s32[]{:S(2)}) async-start(), calls=%async_computation.2 | async-start | bytes 25952256 | tf_op jit(solution)/shard_map/all_gather | solution.py:27
  14.4 0.9 copy-start.4
  17.4 30.7 %all-to-all-start = ((bf16[4,128,2048]{2,1,0:T(8,128)(2,1)}), bf16[4,128,2048]{2,1,0:T(8,128)(2,1)S(1)}, u32[]{:S(2)}, u32[]{:S(2)}) async-start(bf16[4,128,2048]{2,1,0:T(8,128)(2,1)} %broadcast_in_dim.18), calls=%async_computation | async-start | bytes 4194304 | tf_op jit(solution)/shard_map/all_to_all | solution.py:32
  21.8 120.3 %all-gather.15.cloned.1.call-start = ((), (), s32[]{:S(2)}) async-start(), calls=%async_computation.6 | async-start | bytes 3145728 | tf_op jit(solution)/shard_map/all_gather | solution.py:57
  21.8 91.1 %copy-start.25 = (f32[2]{0:T(128)}, f32[2]{0:T(128)S(1)}, u32[]{:S(2)}) copy-start(f32[2]{0:T(128)S(1)} %add_multiply_fusion) | copy-start | bytes 28
  48.1 171.0 %copy-start = (bf16[4,128,2048]{2,1,0:T(8,128)(2,1)}, bf16[4,128,2048]{2,1,0:T(8,128)(2,1)S(1)}, u32[]{:S(2)}) copy-start(bf16[4,128,2048]{2,1,0:T(8,128)(2,1)S(1)} %all-to-all-done) | copy-start | bytes 6291460
  121.8 4.9 %copy-start.6 = (f32[512,2,128]{2,0,1:T(8,128)}, f32[512,2,128]{2,0,1:T(8,128)S(1)}, u32[]{:S(2)}) copy-start(f32[512,2,128]{2,0,1:T(8,128)S(1)} %get-tuple-element.9) | copy-start | bytes 1572868
  121.8 4.9 %copy-start.7 = (f32[512,2,128]{2,0,1:T(8,128)}, f32[512,2,128]{2,0,1:T(8,128)S(1)}, u32[]{:S(2)}) copy-start(f32[512,2,128]{2,0,1:T(8,128)S(1)} %get-tuple-element.10) | copy-start | bytes 1572868
  126.7 1.0 copy-start.27
  129.4 65.3 %all-gather.11.cloned.1.call-start = ((), (), s32[]{:S(2)}) async-start(), calls=%async_computation.3 | async-start | bytes 5242880 | tf_op jit(solution)/shard_map/all_gather | solution.py:57
  131.2 13.7 %copy-start.15 = (f32[2]{0:T(128)}, f32[2]{0:T(128)S(1)}, u32[]{:S(2)}) copy-start(f32[2]{0:T(128)S(1)} %get-tuple-element.63) | copy-start | bytes 28
  141.5 3.4 %copy-start.13 = (f32[2]{0:T(128)}, f32[2]{0:T(128)S(1)}, u32[]{:S(2)}) copy-start(f32[2]{0:T(128)S(1)} %get-tuple-element.61) | copy-start | bytes 28
  141.5 53.1 %copy-start.11 = (f32[2]{0:T(128)}, f32[2]{0:T(128)S(1)}, u32[]{:S(2)}) copy-start(f32[2]{0:T(128)S(1)} %get-tuple-element.60) | copy-start | bytes 28
  144.9 102.4 %all-gather.13.cloned.1.call-start = ((), (), s32[]{:S(2)}) async-start(), calls=%async_computation.4 | async-start | bytes 5242880 | tf_op jit(solution)/shard_map/all_gather | solution.py:57
  145.0 53.4 %copy-start.17 = (f32[2]{0:T(128)}, f32[2]{0:T(128)S(1)}, u32[]{:S(2)}) copy-start(f32[2]{0:T(128)S(1)} %get-tuple-element.57) | copy-start | bytes 28
  145.0 53.4 %copy-start.19 = (f32[2]{0:T(128)}, f32[2]{0:T(128)S(1)}, u32[]{:S(2)}) copy-start(f32[2]{0:T(128)S(1)} %get-tuple-element.58) | copy-start | bytes 28
  145.0 53.4 %copy-start.21 = (f32[2]{0:T(128)}, f32[2]{0:T(128)S(1)}, u32[]{:S(2)}) copy-start(f32[2]{0:T(128)S(1)} %get-tuple-element.59) | copy-start | bytes 28
  198.4 106.5 %reduce-scatter.2.cloned.1.call-start = ((), (), s32[]{:S(2)}) async-start(), calls=%async_computation.5 | async-start | bytes 2621440 | tf_op jit(solution)/shard_map/reduce_scatter | solution.py:256
  219.1 5.2 %copy-start.8 = (bf16[512,2,128]{2,0,1:T(8,128)(2,1)S(1)}, bf16[512,2,128]{2,0,1:T(8,128)(2,1)}, u32[]{:S(2)}) copy-start(bf16[512,2,128]{2,0,1:T(8,128)(2,1)} %get-tuple-element.13) | copy-start | bytes 786436
  222.0 0.8 copy-start.5
  222.8 5.8 %collective-permute-start = (bf16[30,512]{1,0:T(8,128)(2,1)S(1)}, bf16[30,512]{1,0:T(8,128)(2,1)S(1)}, u32[]{:S(2)}, u32[]{:S(2)}) collective-permute-start(bf16[30,512]{1,0:T(8,128)(2,1)S(1)} %slice.380), channel_id=1, source_target_pairs={{0,4},{4,8},{8,12},{12,16},{16,20},{20,24},{24,28},{28,32},{32,36}... | collective-permute-start | bytes 92168 | tf_op jit(solution)/shard_map/ppermute | solution.py:70
  228.6 18.8 %copy-start.2 = (f32[4,256,512]{2,1,0:T(8,128)S(1)}, f32[4,256,512]{2,1,0:T(8,128)}, u32[]{:S(2)}) copy-start(f32[4,256,512]{2,1,0:T(8,128)} %all-gather.15.cloned.1.call-done) | copy-start | bytes 6291460
  228.6 18.8 %copy-start.10 = (f32[512,2]{0,1:T(2,128)S(1)}, f32[512,2]{0,1:T(2,128)}, u32[]{:S(2)}) copy-start(f32[512,2]{0,1:T(2,128)} %get-tuple-element.64) | copy-start | bytes 12292
  228.6 18.8 %copy-start.12 = (f32[2]{0:T(128)S(1)}, f32[2]{0:T(128)}, u32[]{:S(2)}) copy-start(f32[2]{0:T(128)} %copy-done.11) | copy-start | bytes 28
  228.6 18.7 %copy-start.14 = (f32[2]{0:T(128)S(1)}, f32[2]{0:T(128)}, u32[]{:S(2)}) copy-start(f32[2]{0:T(128)} %copy-done.13) | copy-start | bytes 28
  228.6 18.7 %copy-start.16 = (f32[2]{0:T(128)S(1)}, f32[2]{0:T(128)}, u32[]{:S(2)}) copy-start(f32[2]{0:T(128)} %copy-done.15) | copy-start | bytes 28
  228.6 18.7 %copy-start.18 = (f32[2]{0:T(128)S(1)}, f32[2]{0:T(128)}, u32[]{:S(2)}) copy-start(f32[2]{0:T(128)} %copy-done.17) | copy-start | bytes 28
  228.6 18.7 %copy-start.20 = (f32[2]{0:T(128)S(1)}, f32[2]{0:T(128)}, u32[]{:S(2)}) copy-start(f32[2]{0:T(128)} %copy-done.19) | copy-start | bytes 28
  228.6 18.7 %copy-start.22 = (f32[2]{0:T(128)S(1)}, f32[2]{0:T(128)}, u32[]{:S(2)}) copy-start(f32[2]{0:T(128)} %copy-done.21) | copy-start | bytes 28
  228.7 18.7 %copy-start.26 = (f32[2]{0:T(128)S(1)}, f32[2]{0:T(128)}, u32[]{:S(2)}) copy-start(f32[2]{0:T(128)} %get-tuple-element.7) | copy-start | bytes 28
  255.8 11.6 %copy-start.1 = (bf16[4,128,2048]{2,1,0:T(8,128)(2,1)S(1)}, bf16[4,128,2048]{2,1,0:T(8,128)(2,1)}, u32[]{:S(2)}) copy-start(bf16[4,128,2048]{2,1,0:T(8,128)(2,1)} %copy-done) | copy-start | bytes 6291460
  255.8 11.6 %copy-start.23 = (f32[512]{0:T(512)S(1)}, f32[512]{0:T(512)}, u32[]{:S(2)}) copy-start(f32[512]{0:T(512)} %dynamic_slice.10) | copy-start | bytes 6148
  255.8 11.6 %copy-start.24 = (f32[512]{0:T(512)S(1)}, f32[512]{0:T(512)}, u32[]{:S(2)}) copy-start(f32[512]{0:T(512)} %dynamic_slice.11) | copy-start | bytes 6148
Sparse Core Ops, SparseCore 0:
  15.5 94.5 all-gather.8
  129.5 12.5 all-gather.14
  145.0 49.5 all-gather.10
  198.6 48.7 all-gather.12
  275.0 29.8 reduce-scatter.1
where the time goes:
time: 313 us; the launch traced here: 311 us
  waiting for transfers between devices  168 us (54%)
  matrix products  47.5 us (15%)
  other arithmetic  31.2 us (10%)
  local copies, waits for them, and re-layouts  23.4 us (7%)
  blocking collectives  21.4 us (7%)
  between operations  13.6 us (4%)
  starting transfers between devices  6.01 us (2%)
    all_gather x1, waiting for transfers between devices, in_one_piece(): lax.all_gather(both, axis, axis=dim, tiled=True)  61.9 us
    all_gather x3, waiting for transfers between devices, entering(): pieces = jax.tree.map(lambda part: lax.all_gather(part, axis), total)  52.5 us
    reduce_scatter x1, waiting for transfers between devices, local(): lax.psum_scatter((contract(retain_hidden, retain_full) + contract(convolv...  30 us
    all_to_all x1, waiting for transfers between devices, copy_for_each(): return lax.all_to_all(copies, axis, split_axis=0, concat_axis=0, tiled=True)  23.9 us
    all_gather x3, blocking collectives, entering(): pieces = jax.tree.map(lambda part: lax.all_gather(part, axis), total)  21.4 us
    dot_general x2, matrix products, contract(): lax.dot_general(hidden, matrix, (((1,), (1,)), ((), ())), preferred_eleme...  19.1 us
    dot_general x5, matrix products, project(): jnp.dot(row_piece, matrix, preferred_element_type=jnp.float32)  16.5 us
    reduce_sum x1, other arithmetic, convolve_branch(): average = jnp.mean(grouped, axis=-1, keepdims=True)  16.1 us
  transfers between devices with their start and end apart: 7, of which 6 were waited for; matrix products, arithmetic and copies ran while one was open for 13% of the time, Pallas kernels for 0%

commit v1 on v0

--- a/solution.py
+++ b/solution.py
@@ -1,46 +1,263 @@
+import functools
+
 import jax
 import jax.numpy as jnp
 from jax import lax
-from jax.sharding import Mesh
+from jax.experimental import pallas as pl
+from jax.experimental.pallas import tpu as pltpu
 from jax.sharding import PartitionSpec as P
 
+MESH = pl.DeviceIdType.MESH
 KEY = 256
 VAL = 512
 GROUP = 512
 KW = 31
-SP = ("sp_0", "sp_1", "sp_2")
-SP_TP = ("sp_0", "sp_1", "sp_2", "tp")
-
-
 rms_eps = 1e-06
 group_eps = 1.0
 layer_eps = 0.001
 rope_base = 10000.0
-
-
-def in_one_piece(arrays, axis, dim, along):
-    ends, at = ([], 0)
-    for a in arrays[:-1]:
-        at += a.shape[along]
-        ends.append(at)
-    both = jnp.concatenate(arrays, axis=along)
-    return tuple(jnp.split(lax.all_gather(both, axis, axis=dim, tiled=True), ends, axis=along))
-
-
-def copy_for_each(x, axis):
-    copies = jnp.broadcast_to(x, (lax.axis_size(axis), *x.shape))
-    return lax.all_to_all(copies, axis, split_axis=0, concat_axis=0, tiled=True)
-
-
-def in_order(parts, dim):
-    parts = jnp.moveaxis(parts, 0, dim)
-    lengths = parts.shape
-    return parts.reshape(*lengths[:dim], lengths[dim] * lengths[dim + 1], *lengths[dim + 2 :])
-
-
-def gather_directly(x, axis, dim):
-    parts = copy_for_each(x, axis)
-    return in_order(parts, dim)
+HOPS = (0, 3, 1, 2)
+
+
+def body(
+    tok,
+    gain,
+    wq,
+    wk,
+    wv,
+    wrg,
+    wuv,
+    wug,
+    wcg,
+    wro,
+    wco,
+    p0,
+    p1,
+    p2,
+    w3,
+    W,
+    N,
+    tokv,
+    gainv,
+    PV,
+    lsem,
+    wss,
+    wrs,
+    nss,
+    nrs,
+    osem,
+):
+    sp = lax.axis_index("sp")
+    x = lax.axis_index("tp")
+    c = sp % 2
+    y = (sp // 2) % 4
+    z = sp // 8
+
+    def coords(k1, k2, cc):
+        ky = k1 * (1 - cc) + k2 * cc
+        kz = k2 * (1 - cc) + k1 * cc
+        return (z + kz) % 4, (y + ky) % 4
+
+    def device(k1, k2):
+        zz, yy = coords(k1, k2, c)
+        return ((zz * 4 + yy) * 2 + c, x)
+
+    n1p, n1m, n2p, n2m = device(1, 0), device(3, 0), device(0, 1), device(0, 3)
+    partner = ((z * 4 + y) * 2 + 1 - c, x)
+    xp, xm = (sp, (x + 1) % 4), (sp, (x + 3) % 4)
+
+    def block(g, k1, k2, lo=0, rows=64):
+        zz, yy = coords(k1, k2, c)
+        return W.at[g, zz, yy, c, pl.ds(lo, rows), :]
+
+    def other(g, k1, k2):
+        zz, yy = coords(k1, k2, 1 - c)
+        return W.at[g, zz, yy, 1 - c]
+
+    loads = []
+
+    def load(src, dst, i):
+        cp = pltpu.make_async_copy(src, dst, lsem.at[i])
+        cp.start()
+        loads.append(cp)
+
+    load(tok, tokv, 0)
+    load(gain, gainv, 1)
+    own = lambda g, a, b: W.at[g, z, y, c, :, pl.ds(a, b)]
+    load(wk, own(0, 0, 512), 2)
+    load(wv, own(0, 512, 1024), 3)
+    load(wq, own(1, 0, 512), 4)
+    load(wuv, own(1, 512, 512), 5)
+    load(wug, own(1, 1024, 512), 6)
+    load(wrg, own(2, 0, 1024), 7)
+    load(wcg, own(2, 1024, 512), 8)
+    load(wro, own(3, 0, 1024), 9)
+    load(wco, own(3, 1024, 512), 10)
+
+    barrier = pltpu.get_barrier_semaphore()
+    for dev in (n1p, n1m, n2p, n2m, partner, xp, xm):
+        pl.semaphore_signal(barrier, inc=1, device_id=dev, device_id_type=MESH)
+    for cp in loads[2:4]:
+        cp.wait()
+    pl.semaphore_wait(barrier, 7)
+
+    sends = []
+
+    def remote(ref, ss, rs, dev):
+        return pltpu.make_async_remote_copy(
+            src_ref=ref, dst_ref=ref, send_sem=ss, recv_sem=rs, device_id=dev, device_id_type=MESH
+        )
+
+    def wsend(ref, g, i, dev):
+        cp = remote(ref, wss.at[g, i], wrs.at[g, i], dev)
+        cp.start()
+        sends.append(cp)
+
+    def wwait(ref, g, i):
+        remote(ref, wss.at[g, i], wrs.at[g, i], partner).wait_recv()
+
+    def s1(g):
+        wsend(block(g, 0, 0), g, 0, n1p)
+        wsend(block(g, 0, 0), g, 1, n1m)
+
+    def s2(g):
+        wwait(block(g, 3, 0), g, 0)
+        wsend(block(g, 3, 0, 0, 32), g, 2, n1p)
+        wwait(block(g, 1, 0), g, 1)
+        wsend(block(g, 1, 0, 32, 32), g, 3, n1m)
+
+    def s3(g):
+        for j in range(3):
+            k = HOPS[j]
+            wsend(block(g, k, 0), g, 4 + j, n2p)
+            wsend(block(g, k, 0), g, 8 + j, n2m)
+            wsend(block(g, k, 0), g, 20 + j, partner)
+
+    def s3b(g):
+        wwait(block(g, 2, 0, 0, 32), g, 2)
+        wwait(block(g, 2, 0, 32, 32), g, 3)
+        wsend(block(g, 2, 0), g, 7, n2p)
+        wsend(block(g, 2, 0), g, 11, n2m)
+        wsend(block(g, 2, 0), g, 23, partner)
+
+    def s4(g, j):
+        k = HOPS[j]
+        wwait(block(g, k, 3), g, 4 + j)
+        wsend(block(g, k, 3, 0, 32), g, 12 + j, n2p)
+        wsend(block(g, k, 3), g, 24 + j, partner)
+        wwait(block(g, k, 1), g, 8 + j)
+        wsend(block(g, k, 1, 32, 32), g, 16 + j, n2m)
+        wsend(block(g, k, 1), g, 28 + j, partner)
+
+    def s5(g, j):
+        k = HOPS[j]
+        wwait(block(g, k, 2, 0, 32), g, 12 + j)
+        wwait(block(g, k, 2, 32, 32), g, 16 + j)
+        wsend(block(g, k, 2), g, 32 + j, partner)
+
+    def s6(g):
+        for j in range(4):
+            for q, k2 in enumerate((0, 3, 1, 2)):
+                wwait(other(g, HOPS[j], k2), g, 20 + 4 * q + j)
+
+    s1(0)
+    loads[0].wait()
+    loads[1].wait()
+    tk = tokv[...].astype(jnp.float32)
+    scale = lax.rsqrt(jnp.mean(tk * tk, axis=-1, keepdims=True) + rms_eps)
+    N[x] = (tk * scale * gainv[...]).astype(jnp.bfloat16)
+    for cp in loads[4:]:
+        cp.wait()
+    s1(1)
+    s2(0)
+
+    def nsend(ref, i, dev):
+        cp = remote(ref, nss.at[i], nrs.at[i], dev)
+        cp.start()
+        sends.append(cp)
+
+    def nwait(ref, i):
+        remote(ref, nss.at[i], nrs.at[i], partner).wait_recv()
+
+    nsend(N.at[x], 0, xp)
+    nsend(N.at[x], 1, xm)
+
+    def project(g, n):
+        cols = pl.ds(pl.multiple_of(n * 256, 256), 256)
+        w = W[g, :, :, :, :, cols].reshape(2048, 256)
+        lhs = N[...].reshape(512, 2048)
+        PV[g, :, cols] = jnp.dot(lhs, w, preferred_element_type=jnp.float32).astype(jnp.bfloat16)
+
+    outs = (p0, p1, p2)
+    for g in range(4):
+        s3(g)
+        if g + 2 < 4:
+            s1(g + 2)
+        s3b(g)
+        if g + 1 < 4:
+            s2(g + 1)
+        if g == 0:
+            xl, xr = (x + 3) % 4, (x + 1) % 4
+            nwait(N.at[xl], 0)
+            nsend(N.at[xl, pl.ds(0, 64), :], 2, xp)
+            nwait(N.at[xr], 1)
+            nsend(N.at[xr, pl.ds(64, 64), :], 3, xm)
+        for j in range(4):
+            s4(g, j)
+            if g > 0 and j < 3:
+
+                def step(i, carry, g=g, j=j):
+                    project(g - 1, j * 2 + i)
+                    return carry
+
+                lax.fori_loop(0, 2, step, 0)
+        if g > 0:
+            cp = pltpu.make_async_copy(PV.at[g - 1], outs[g - 1], osem.at[g - 1])
+            cp.start()
+            loads.append(cp)
+        for j in range(4):
+            s5(g, j)
+        if g == 0:
+            xf = (x + 2) % 4
+            nwait(N.at[xf, pl.ds(0, 64), :], 2)
+            nwait(N.at[xf, pl.ds(64, 64), :], 3)
+        s6(g)
+    cp = pltpu.make_async_copy(W.at[3], w3, osem.at[3])
+    cp.start()
+    cp.wait()
+    for cp in loads[11:]:
+        cp.wait()
+    for cp in sends:
+        cp.wait_send()
+
+
+def gather_project(tokens, norm_gain, *ws):
+    any_spec = pl.BlockSpec(memory_space=pl.ANY)
+    bf = jnp.bfloat16
+    return pl.pallas_call(
+        body,
+        out_shape=[jax.ShapeDtypeStruct((512, 1536), bf)] * 3
+        + [jax.ShapeDtypeStruct((4, 4, 2, 64, 1536), bf)],
+        in_specs=[any_spec] * 11,
+        out_specs=[any_spec] * 4,
+        scratch_shapes=[
+            pltpu.VMEM((4, 4, 4, 2, 64, 1536), bf),
+            pltpu.VMEM((4, 128, 2048), bf),
+            pltpu.VMEM((128, 2048), bf),
+            pltpu.VMEM((1, 2048), jnp.float32),
+            pltpu.VMEM((3, 512, 1536), bf),
+            pltpu.SemaphoreType.DMA((11,)),
+            pltpu.SemaphoreType.DMA((4, 36)),
+            pltpu.SemaphoreType.DMA((4, 36)),
+            pltpu.SemaphoreType.DMA((4,)),
+            pltpu.SemaphoreType.DMA((4,)),
+            pltpu.SemaphoreType.DMA((4,)),
+        ],
+        compiler_params=pltpu.CompilerParams(
+            collective_id=0, has_side_effects=True, vmem_limit_bytes=56 * 1024 * 1024
+        ),
+        name="gather_project",
+    )(tokens, norm_gain, *ws)
 
 
 def filled_with(x, identity):
@@ -68,12 +285,6 @@
     length = lax.axis_size(axis)
     pairs = [(i, i + by) for i in range(length) if 0 <= i + by < length]
     return lax.ppermute(x, axis, pairs)
-
-
-def rms_normalize(tokens, norm_gain):
-    widened = tokens.astype(jnp.float32)
-    scaled = widened * lax.rsqrt(jnp.mean(widened * widened, axis=-1, keepdims=True) + rms_eps)
-    return (scaled * norm_gain).astype(jnp.bfloat16)
 
 
 def rotate(vectors, positions):
@@ -168,63 +379,27 @@
     return (earlier[0] * later[0], later[0][:, None, None] * earlier[1] + later[1])
 
 
-def local(
-    tokens,
-    norm_gain,
-    query_weight,
-    key_weight,
-    value_weight,
-    retain_gate,
-    unit_value,
-    unit_gate,
-    convolve_gate,
-    filter_taps,
-    layer_gain,
-    layer_shift,
-    retain_output,
-    convolve_output,
-):
+SP = ("sp_0", "sp_1", "sp_2")
+SP_TP = ("sp_0", "sp_1", "sp_2", "tp")
+
+
+def local_a(tokens, norm_gain, query_weight, key_weight, value_weight, retain_gate, unit_value, unit_gate, convolve_gate, retain_output, convolve_output):
+    return tuple(gather_project(
+        tokens, norm_gain.reshape(1, -1), query_weight, key_weight, value_weight, retain_gate,
+        unit_value, unit_gate, convolve_gate, retain_output, convolve_output,
+    ))
+
+
+def local_b(p0, p1, p2, w3, filter_taps, layer_gain, layer_shift):
     head_groups = lax.axis_size("tp")
     chain_length = lax.axis_size(SP)
     head_rank = lax.axis_index("tp")
     chain_rank = lax.axis_index(SP)
-    normed = rms_normalize(tokens, norm_gain)
-    gathered = in_one_piece(
-        (
-            query_weight,
-            key_weight,
-            value_weight,
-            retain_gate,
-            unit_value,
-            unit_gate,
-            convolve_gate,
-            retain_output,
-            convolve_output,
-        ),
-        SP,
-        0,
-        1,
-    )
-    in_weights = gathered[:7]
-    retain_full = gathered[7]
-    convolve_full = gathered[8]
-
-    def project(row_piece):
-        return jnp.concatenate(
-            [
-                jnp.dot(row_piece, matrix, preferred_element_type=jnp.float32).astype(jnp.bfloat16)
-                for matrix in in_weights
-            ],
-            axis=1,
-        )
-
-    projected = project(gather_directly(normed, "tp", 0))
-    row_count = projected.shape[0]
-    bounds = [0]
-    for matrix in in_weights:
-        bounds.append(bounds[-1] + matrix.shape[1])
-    pieces = [projected[:, bounds[column] : bounds[column + 1]] for column in range(7)]
-    queries, key_rows, values, retain_switch, glu_value, glu_switch, convolve_switch = pieces
+    key_rows, values = p0[:, :512], p0[:, 512:]
+    queries, glu_value, glu_switch = p1[:, :512], p1[:, 512:1024], p1[:, 1024:]
+    retain_switch, convolve_switch = p2[:, :1024], p2[:, 1024:]
+    w3 = w3.reshape(2048, 1536)
+    row_count = 512
     local_heads = queries.shape[1] // KEY
     positions = chain_rank * row_count + jnp.arange(row_count, dtype=jnp.int32)
     rotated_query, rotated_keys, value_heads = prepare(queries, key_rows, values, positions)
@@ -254,7 +429,7 @@
         gated_input, before, tap_slice, gain_slice, shift_slice, convolve_switch
     )
     return lax.psum_scatter(
-        (contract(retain_hidden, retain_full) + contract(convolve_hidden, convolve_full)).astype(
+        contract(jnp.concatenate([retain_hidden, convolve_hidden], axis=1), w3).astype(
             jnp.bfloat16
         ),
         "tp",
@@ -264,23 +439,29 @@
 
 
 def solution(mesh):
+    from jax.sharding import Mesh
+
     finer = Mesh(mesh.devices.reshape(4, 4, 2, mesh.shape["tp"]), ("sp_0", "sp_1", "sp_2", "tp"))
-    placed = (
-        P(SP_TP, None),
-        P(),
-        P(SP, "tp"),
-        P(SP, "tp"),
-        P(SP, "tp"),
-        P(SP, "tp"),
-        P(SP, "tp"),
-        P(SP, "tp"),
-        P(SP, "tp"),
-        P(),
-        P(),
-        P(),
-        P(SP, "tp"),
-        P(SP, "tp"),
-    )
-    return jax.shard_map(
-        local, mesh=finer, in_specs=placed, out_specs=P(SP_TP, None), check_vma=False
-    )
+    weight = P("sp", "tp")
+    rows = P(("sp", "tp"), None)
+    first = jax.shard_map(
+        local_a,
+        mesh=mesh,
+        in_specs=(rows, P()) + (weight,) * 9,
+        out_specs=(weight,) * 3 + (P("sp", "tp"),),
+        check_vma=False,
+    )
+    fine = P(SP, "tp")
+    second = jax.shard_map(
+        local_b,
+        mesh=finer,
+        in_specs=(fine,) * 3 + (fine,) + (P(),) * 3,
+        out_specs=P(SP_TP, None),
+        check_vma=False,
+    )
+
+    def run(tokens, norm_gain, qw, kw, vw, rg, uv, ug, cg, taps, lg, ls, ro, co):
+        p0, p1, p2, w3 = first(tokens, norm_gain, qw, kw, vw, rg, uv, ug, cg, ro, co)
+        return second(p0, p1, p2, w3, taps, lg, ls)
+
+    return run

time: 313 us -> 282 us (0.901)
  Pallas kernels: 0 us -> 92 us
  waiting for transfers between devices: 168 us -> 101 us
  matrix products: 47.5 us -> 18.9 us
  local copies, waits for them, and re-layouts: 23.4 us -> 11.4 us
  other arithmetic: 31.2 us -> 21.3 us
  starting transfers between devices: 6.01 us -> 1.88 us
    pallas_call x0 -> x1, Pallas kernels: none -> 92 us  [gather_project(): pl.pallas_call(body, out_shape=[jax.ShapeDtypeStruct((512, 1536), bf)] *...]
    all_gather x1 -> x0, waiting for transfers between devices: 61.9 us -> none  [in_one_piece(): lax.all_gather(both, axis, axis=dim, tiled=True)]
    all_to_all x1 -> x0, waiting for transfers between devices: 23.9 us -> none  [copy_for_each(): return lax.all_to_all(copies, axis, split_axis=0, concat_axis=0, tiled=True)]
    all_gather x3, waiting for transfers between devices: 52.5 us -> 70.7 us  [entering(): pieces = jax.tree.map(lambda part: lax.all_gather(part, axis), total)]
    dot_general x5 -> x0, matrix products: 16.5 us -> none  [project(): jnp.dot(row_piece, matrix, preferred_element_type=jnp.float32)]
    unnamed x68 -> x24, local copies, waits for them, and re-layouts: 13 us -> 0.25 us
    dot_general x2 -> x1, matrix products: 19.1 us -> 7.54 us  [contract(): lax.dot_general(hidden, matrix, (((1,), (1,)), ((), ())), preferred_eleme...]
    reduce_sum x1, other arithmetic: 16.1 us -> 4.65 us  [convolve_branch(): average = jnp.mean(grouped, axis=-1, keepdims=True)]
  transfers between devices with their start and end apart: 7 -> 5, of which waited for: 6 -> 4; matrix products, arithmetic and copies ran while one was open for 13% -> 6% of each run, Pallas kernels for 0% -> 0%
where the time goes in v1:
time: 282 us; the launch traced here: 281 us
  waiting for transfers between devices  101 us (36%)
  Pallas kernels  92 us (33%)
  other arithmetic  21.3 us (8%)
  blocking collectives  21 us (7%)
  matrix products  18.9 us (7%)
  between operations  13.4 us (5%)
  local copies, waits for them, and re-layouts  11.4 us (4%)
    pallas_call x1, Pallas kernels, gather_project(): pl.pallas_call(body, out_shape=[jax.ShapeDtypeStruct((512, 1536), bf)] *...  92 us
    all_gather x3, waiting for transfers between devices, entering(): pieces = jax.tree.map(lambda part: lax.all_gather(part, axis), total)  70.7 us
    reduce_scatter x1, waiting for transfers between devices, local_b(): lax.psum_scatter(contract(jnp.concatenate([retain_hidden, convolve_hidden...  30 us
    all_gather x3, blocking collectives, entering(): pieces = jax.tree.map(lambda part: lax.all_gather(part, axis), total)  21 us
    dot_general x1, matrix products, contract(): lax.dot_general(hidden, matrix, (((1,), (1,)), ((), ())), preferred_eleme...  7.54 us
    add x2, other arithmetic, join_states(): later[0][:, None, None] * earlier[1] + later[1]  6.66 us
    dot_general x1, matrix products, cross_part(): jnp.einsum('ihd,hde->ihe', queries.astype(jnp.float32), carry_state)  5.87 us
  transfers between devices with their start and end apart: 5, of which 4 were waited for; matrix products, arithmetic and copies ran while one was open for 6% of the time, Pallas kernels for 0%

profile of v1, /device:TPU:0, one launch (start us, length us, event | category | flops | bytes accessed | tf_op | source)
XLA Modules:
  0.0 280.8 jit_solution(8136613452021067504)
XLA Ops:
  6.5 0.0 all-gather.12.cloned.1.call-start
  6.6 92.0 %gather_project.1 = (bf16[512,1536]{1,0:T(8,128)(2,1)}, bf16[512,1536]{1,0:T(8,128)(2,1)}, bf16[512,1536]{1,0:T(8,128)(2,1)}, bf16[4,4,2,64,1536]{4,3,2,1,0:T(8,128)(2,1)}) custom-call(bf16[128,2048]{1,0:T(8,128)(2,1)} %tok.1, f32[1,2048]{1,0:T(1,128)} %bitcast.172, bf16[64,512]{1,0:T(8,128)(2,1)} %wq.1, bf16[64,512]{1,0:T(8,128)(2,1)} %wk.1, ...), custom_call_target="tpu_custom_call" | custom-call | tf_op jit(solution)/shard_map/gather_project/pallas_call | solution.py:237
  98.6 2.3 slice.285
  101.0 1.5 slice_convert_fusion
  102.5 0.7 reshape.316
  103.1 1.3 fusion.137
  104.5 0.7 reshape.314
  105.2 0.4 fusion.138
  105.5 1.0 multiply_cosine_fusion
  106.5 0.1 multiply_exponential_fusion
  106.6 0.0 copy-done.1
  106.6 0.0 copy-done.2
  106.6 0.0 copy-start.4
  106.6 1.0 multiply_subtract_fusion
  107.6 0.2 copy-done.4
  107.8 1.6 fusion.15
  109.5 0.0 all-gather.12.cloned.1.call-update
  109.5 0.0 copy-done.6
  109.5 0.0 all-gather.8.cloned.1.call-start
  109.6 2.1 all-gather.1
  111.7 8.6 %all-gather.2 = f32[4,1,2]{2,1,0:T(1,128)S(1)} all-gather(f32[1,1,2]{2,1,0:T(1,128)S(1)} %get-tuple-element.66), channel_id=1, replica_groups=mesh['sp_0'=4,'sp_1'=4,'sp_2'=2,'tp'=4] {'sp_1'}, dimensions={0}, use_global_device_ids=true | all-gather | bytes 40 | tf_op jit(solution)/shard_map/all_gather | solution.py:274
  120.3 0.1 all-gather.12.cloned.1.call-done
  120.4 2.8 %bitcast_add_fusion.4 = f32[1,2,256,512]{3,2,1,0:T(8,128)} fusion(f32[4,256,512]{2,1,0:T(8,128)} %all-gather.12.cloned.1.call-done, f32[2]{0:T(128)S(1)} %get-tuple-element.65, f32[2]{0:T(128)S(1)} %get-tuple-element.67), kind=kLoop, calls=%fused_computation.75 | loop fusion | flops 786432 | bytes 3145744 | tf_op jit(solution)/shard_map/add | solution.py:379
  123.2 0.0 all-gather.8.cloned.1.call-update
  123.2 0.2 all-gather.10.cloned.1.call-start
  123.5 49.5 %all-gather.8.cloned.1.call-done = f32[4,2,256,512]{3,2,1,0:T(8,128)} async-done(((f32[1,2,256,512]{3,2,1,0:T(8,128)}), f32[4,2,256,512]{3,2,1,0:T(8,128)}) %all-gather.8.cloned.1.call-update) | async-done | bytes 4194320 | tf_op jit(solution)/shard_map/all_gather | solution.py:274
  173.0 0.0 copy-done.5
  173.0 3.8 %multiply_add_fusion.1 = f32[1,2,256,512]{3,2,1,0:T(8,128)} fusion(f32[4,2,256,512]{3,2,1,0:T(8,128)} %all-gather.8.cloned.1.call-done, f32[2]{0:T(128)S(1)} %get-tuple-element.64, f32[2]{0:T(128)S(1)} %get-tuple-element.63, f32[2]{0:T(128)S(1)} %get-tuple-element.62, f32[2]{0:T(128)S(1)} %get-tuple-element.61), kind=kLoop, calls=%fused_computation.98 | loop fusion | flops 1835008 | bytes 5242912 | tf_op jit(solution)/shard_map/add | solution.py:379
  176.8 0.0 all-gather.10.cloned.1.call-update
  176.8 0.0 reduce-scatter.2.cloned.1.call-start
  176.9 0.0 copy-done.3
  176.9 0.3 multiply_convert_fusion.1
  177.2 1.6 collective-permute-start
  178.8 10.3 %all-gather.3 = f32[4,1,2]{2,1,0:T(1,128)S(1)} all-gather(f32[1,1,2]{2,1,0:T(1,128)S(1)} %get-tuple-element.60), channel_id=1, replica_groups=mesh['sp_0'=4,'sp_1'=4,'sp_2'=2,'tp'=4] {'sp_0'}, dimensions={0}, use_global_device_ids=true | all-gather | bytes 40 | tf_op jit(solution)/shard_map/all_gather | solution.py:274
  189.1 1.1 constant_dynamic-slice_fusion
  190.2 0.3 fusion.55
  190.5 0.2 fusion.54
  190.7 0.6 slice_bitcast_fusion.6
  191.3 3.9 %fusion.9 = f32[2,512,512]{1,2,0:T(8,128)} fusion(f32[512,512]{1,0:T(8,128)S(1)} %fusion.54, f32[2]{0:T(128)S(1)} %add_multiply_fusion, pred[512,512]{1,0:T(8,128)(4,1)S(1)} %fusion.55, bf16[64,2,8,512]{3,2,1,0:T(8,128)(2,1)S(1)} %bitcast.171, bf16[512,2,128]{2,0,1:T(8,128)(2,1)S(1)} %get-tuple-element.21, bf16[512,2,128]{2,0,1:T(8,128)(2,1)} %get-tuple-element.22, ...), kind=kOutput, calls=%fused_computation.45 | convolution fusion | flops 809238528 | bytes 6029320 | tf_op jit(solution)/shard_map/hij,jhe->ihe/dot_general | solution.py:332
  195.2 1.2 fusion.139
  196.4 0.8 dynamic_slice.10
  197.2 0.8 dynamic_slice.11
  197.9 0.0 collective-permute-done
  197.9 4.7 %fusion.136 = (f32[512]{0:T(512)S(1)}, f32[512,512]{1,0:T(8,128)S(1)}) fusion(f32[512]{0:T(512)S(1)} %bitcast.203, bf16[512,512]{1,0:T(8,128)(2,1)S(1)} %multiply_convert_fusion.1, f32[512]{0:T(512)S(1)} %bitcast.174, bf16[30,512]{1,0:T(8,128)(2,1)S(1)} %collective-permute-done, f32[512]{0:T(512)S(1)} %bitcast.175, f32[512]{0:T(512)S(1)} %bitcast.176, ...), kind=kLoop, calls=%fused_computation.228 | loop fusion | flops 47971840 | bytes 1669120 | tf_op jit(solution)/shard_map/reduce_sum | solution.py:365
  202.6 0.0 copy-start.7
  202.6 0.0 copy-start.9
  202.6 0.0 copy-start.10
  202.6 0.0 copy-start.11
  202.7 0.3 multiply_reduce_fusion.1
  202.9 1.7 fusion.56
  204.6 21.1 %all-gather.10.cloned.1.call-done = f32[4,2,256,512]{3,2,1,0:T(8,128)} async-done(((f32[1,2,256,512]{3,2,1,0:T(8,128)}), f32[4,2,256,512]{3,2,1,0:T(8,128)}) %all-gather.10.cloned.1.call-update) | async-done | bytes 4194320 | tf_op jit(solution)/shard_map/all_gather | solution.py:274
  225.7 0.0 copy-done
  225.7 0.0 copy-done.8
  225.8 0.0 copy-done.7
  225.8 0.0 copy-done.10
  225.8 0.0 copy-done.11
  225.8 5.9 %fusion.140 = (f32[512,2]{0,1:T(2,128)S(1)}, f32[512,2,512]{0,2,1:T(8,128)S(1)}) fusion(f32[512,2]{0,1:T(2,128)S(1)} %get-tuple-element.68, bf16[512,2,128]{2,0,1:T(8,128)(2,1)S(1)} %get-tuple-element.21, bf16[512,2,128]{2,0,1:T(8,128)(2,1)S(1)} %copy-done.7, f32[4,2,256,512]{3,2,1,0:T(8,128)} %all-gather.10.cloned.1.call-done, ...), kind=kOutput, calls=%fused_computation.232 | convolution fusion | flops 279182336 | bytes 15212650 | tf_op jit(solution)/shard_map/ihd,hde->ihe/dot_general | solution.py:344
  231.7 0.3 multiply_reduce_fusion
  231.9 0.3 subtract_multiply_fusion
  232.2 1.9 copy.43
  234.1 2.5 fusion.5
  236.7 7.5 %convolution_convert_fusion = bf16[512,2048]{1,0:T(8,128)(2,1)} fusion(bf16[2048,1536]{1,0:T(8,128)(2,1)} %bitcast.204, bf16[512,512]{1,0:T(8,128)(2,1)S(1)} %fusion.56, bf16[512,1024]{1,0:T(8,128)(2,1)S(1)} %fusion.5), kind=kOutput, calls=%fused_computation.29 | convolution fusion | flops 3225419776 | bytes 9961472 | tf_op jit(solution)/shard_map/dot_general | solution.py:373
  244.2 0.0 reduce-scatter.2.cloned.1.call-update
  244.3 30.0 %reduce-scatter.2.cloned.1.call-done = bf16[128,2048]{1,0:T(8,128)(2,1)} async-done(((bf16[512,2048]{1,0:T(8,128)(2,1)}), bf16[128,2048]{1,0:T(8,128)(2,1)}) %reduce-scatter.2.cloned.1.call-update) | async-done | bytes 524304 | tf_op jit(solution)/shard_map/reduce_scatter | solution.py:431
  (21 shorter events, 0.1 us)
Async XLA Ops:
  6.5 113.9 %all-gather.12.cloned.1.call-start = ((), (), s32[]{:S(2)}) async-start(), calls=%async_computation.4 | async-start | bytes 3145728 | tf_op jit(solution)/shard_map/all_gather | solution.py:274
  104.5 2.1 copy-start.1
  104.5 2.1 copy-start.2
  106.6 1.2 copy-start.4
  107.6 1.8 copy-start.6
  107.6 65.3 %copy-start.5 = (f32[512,2,128]{2,0,1:T(8,128)}, f32[512,2,128]{2,0,1:T(8,128)S(1)}, u32[]{:S(2)}) copy-start(f32[512,2,128]{2,0,1:T(8,128)S(1)} %get-tuple-element.13) | copy-start | bytes 1572868
  109.5 63.5 %all-gather.8.cloned.1.call-start = ((), (), s32[]{:S(2)}) async-start(), calls=%async_computation.1 | async-start | bytes 5242880 | tf_op jit(solution)/shard_map/all_gather | solution.py:274
  123.2 102.5 %all-gather.10.cloned.1.call-start = ((), (), s32[]{:S(2)}) async-start(), calls=%async_computation.2 | async-start | bytes 5242880 | tf_op jit(solution)/shard_map/all_gather | solution.py:274
  173.0 3.9 %copy-start.3 = (bf16[512,1536]{1,0:T(8,128)(2,1)S(1)}, bf16[512,1536]{1,0:T(8,128)(2,1)}, u32[]{:S(2)}) copy-start(bf16[512,1536]{1,0:T(8,128)(2,1)} %get-tuple-element.6) | copy-start | bytes 4718596
  176.8 97.4 %reduce-scatter.2.cloned.1.call-start = ((), (), s32[]{:S(2)}) async-start(), calls=%async_computation.3 | async-start | bytes 2621440 | tf_op jit(solution)/shard_map/reduce_scatter | solution.py:431
  177.2 20.7 %collective-permute-start = (bf16[30,512]{1,0:T(8,128)(2,1)S(1)}, bf16[30,512]{1,0:T(8,128)(2,1)S(1)}, u32[]{:S(2)}, u32[]{:S(2)}) collective-permute-start(bf16[30,512]{1,0:T(8,128)(2,1)S(1)} %slice.408), channel_id=1, source_target_pairs={{0,4},{4,8},{8,12},{12,16},{16,20},{20,24},{24,28},{28,32},{32,36}... | collective-permute-start | bytes 92168 | tf_op jit(solution)/shard_map/ppermute | solution.py:287
  197.9 27.8 %copy-start = (f32[4,256,512]{2,1,0:T(8,128)S(1)}, f32[4,256,512]{2,1,0:T(8,128)}, u32[]{:S(2)}) copy-start(f32[4,256,512]{2,1,0:T(8,128)} %all-gather.12.cloned.1.call-done) | copy-start | bytes 6291460
  197.9 27.8 %copy-start.8 = (f32[2]{0:T(128)S(1)}, f32[2]{0:T(128)}, u32[]{:S(2)}) copy-start(f32[2]{0:T(128)} %get-tuple-element.56) | copy-start | bytes 28
  202.6 23.2 %copy-start.7 = (bf16[512,2,128]{2,0,1:T(8,128)(2,1)S(1)}, bf16[512,2,128]{2,0,1:T(8,128)(2,1)}, u32[]{:S(2)}) copy-start(bf16[512,2,128]{2,0,1:T(8,128)(2,1)} %get-tuple-element.22) | copy-start | bytes 786436
  202.6 23.1 %copy-start.9 = (f32[2]{0:T(128)S(1)}, f32[2]{0:T(128)}, u32[]{:S(2)}) copy-start(f32[2]{0:T(128)} %get-tuple-element.57) | copy-start | bytes 28
  202.6 23.1 %copy-start.10 = (f32[2]{0:T(128)S(1)}, f32[2]{0:T(128)}, u32[]{:S(2)}) copy-start(f32[2]{0:T(128)} %get-tuple-element.58) | copy-start | bytes 28
  202.6 23.1 %copy-start.11 = (f32[2]{0:T(128)S(1)}, f32[2]{0:T(128)}, u32[]{:S(2)}) copy-start(f32[2]{0:T(128)} %get-tuple-element.59) | copy-start | bytes 28
Sparse Core Ops, SparseCore 0:
  109.6 10.7 all-gather.11
  123.4 49.5 all-gather.7
  177.0 48.7 all-gather.9
  244.4 29.8 reduce-scatter.1

commit v2 on v1

v2 whole, which is shorter than its diff:
```python
import numpy as np

import jax
import jax.numpy as jnp
from jax import lax
from jax.experimental import pallas as pl
from jax.experimental.pallas import tpu as pltpu
from jax.sharding import PartitionSpec as P

MESH = pl.DeviceIdType.MESH
KEY = 256
VAL = 512
KW = 31
SEQ = 16384
HEADS = 8
rms_eps = 1e-06
group_eps = 1.0
layer_eps = 0.001
rope_base = 10000.0
HOPS = (0, 3, 1, 2)
BF = jnp.bfloat16
F32 = jnp.float32


def rotation_tables():
    frequency = rope_base ** (-np.arange(128, dtype=np.float64) / 128)
    fine = np.arange(512)[:, None] * frequency
    coarse = 512 * np.arange(32)[:, None] * frequency
    pair = lambda a: np.stack([np.cos(a), np.sin(a)], axis=1).astype(np.float32)
    return np.moveaxis(pair(fine), 1, 0), pair(coarse)


def silu(a):
    return a / (1.0 + jnp.exp(-a))


def body(
    tok,
    gain,
    wq,
    wk,
    wv,
    wrg,
    wuv,
    wug,
    wcg,
    wro,
    wco,
    taps,
    lgain,
    lshift,
    fine,
    coarse,
    out,
    W,
    N,
    tokv,
    gainv,
    tapv,
    lgainv,
    lshiftv,
    finev,
    coarsev,
    PV,
    ROT,
    WT,
    RK,
    RQ,
    CF,
    PS,
    PC,
    TB,
    TS,
    SZ,
    SB,
    SF,
    STS,
    STM,
    RAW,
    GP,
    HS,
    HR,
    CV,
    HID,
    OP,
    RA,
    RB,
    OUTV,
    lsem,
    wss,
    wrs,
    nss,
    nrs,
    sss,
    srs,
    rss,
    rrs,
    osem,
):
    sp = lax.axis_index("sp")
    x = lax.axis_index("tp")
    c = sp % 2
    y = (sp // 2) % 4
    z = sp // 8

    def coords(k1, k2, cc):
        ky = k1 * (1 - cc) + k2 * cc
        kz = k2 * (1 - cc) + k1 * cc
        return (z + kz) % 4, (y + ky) % 4

    def place(zz, yy):
        return ((zz * 4 + yy) * 2 + c, x)

    def device(k1, k2):
        return place(*coords(k1, k2, c))

    n1p, n1m, n2p, n2m = device(1, 0), device(3, 0), device(0, 1), device(0, 3)
    partner = ((z * 4 + y) * 2 + 1 - c, x)
    xp, xm = (sp, (x + 1) % 4), (sp, (x + 3) % 4)
    after, before = ((sp + 1) % 32, x), ((sp + 31) % 32, x)

    def block(g, k1, k2, lo=0, rows=64):
        zz, yy = coords(k1, k2, c)
        return W.at[g, zz, yy, c, pl.ds(lo, rows), :]

    def other(g, k1, k2):
        zz, yy = coords(k1, k2, 1 - c)
        return W.at[g, zz, yy, 1 - c]

    loads = []

    def load(src, dst):
        cp = pltpu.make_async_copy(src, dst, lsem.at[len(loads)])
        cp.start()
        loads.append(cp)

    mine = pl.ds(pl.multiple_of(x * 512, 512), 512)
    own = lambda g, a, b: W.at[g, z, y, c, :, pl.ds(a, b)]
    load(wk, own(0, 0, 512))
    load(wv, own(0, 512, 1024))
    load(tok, tokv)
    load(gain, gainv)
    load(wq, own(1, 0, 512))
    load(wuv, own(1, 512, 512))
    load(wug, own(1, 1024, 512))
    load(wrg, own(2, 0, 1024))
    load(wcg, own(2, 1024, 512))
    load(wro, own(3, 0, 1024))
    load(wco, own(3, 1024, 512))
    load(taps.at[:, mine], tapv)
    load(lgain.at[:, mine], lgainv)
    load(lshift.at[:, mine], lshiftv)
    load(fine, finev)
    load(coarse.at[sp], coarsev)

    greeted = (n1p, n1m, n2p, n2m, device(2, 0), device(0, 2), partner, xp, xm, after, before)
    barrier = pltpu.get_barrier_semaphore()
    for dev in greeted:
        pl.semaphore_signal(barrier, inc=1, device_id=dev, device_id_type=MESH)
    for cp in loads[:2]:
        cp.wait()
    pl.semaphore_wait(barrier, len(greeted))

    sends = []

    def remote(src, dst, ss, rs, dev):
        return pltpu.make_async_remote_copy(
            src_ref=src, dst_ref=dst, send_sem=ss, recv_sem=rs, device_id=dev, device_id_type=MESH
        )

    def send(src, dst, ss, rs, dev):
        cp = remote(src, dst, ss, rs, dev)
        cp.start()
        sends.append(cp)

    def arrived(ref, ss, rs):
        remote(ref, ref, ss, rs, partner).wait_recv()

    def wsend(ref, g, i, dev):
        send(ref, ref, wss.at[g, i], wrs.at[g, i], dev)

    def wwait(ref, g, i):
        arrived(ref, wss.at[g, i], wrs.at[g, i])

    def s1(g):
        wsend(block(g, 0, 0), g, 0, n1p)
        wsend(block(g, 0, 0), g, 1, n1m)

    def s2(g):
        wwait(block(g, 3, 0), g, 0)
        wsend(block(g, 3, 0, 0, 32), g, 2, n1p)
        wwait(block(g, 1, 0), g, 1)
        wsend(block(g, 1, 0, 32, 32), g, 3, n1m)

    def s3(g):
        for j in range(3):
            k = HOPS[j]
            wsend(block(g, k, 0), g, 4 + j, n2p)
            wsend(block(g, k, 0), g, 8 + j, n2m)
            wsend(block(g, k, 0), g, 20 + j, partner)

    def s3b(g):
        wwait(block(g, 2, 0, 0, 32), g, 2)
        wwait(block(g, 2, 0, 32, 32), g, 3)
        wsend(block(g, 2, 0), g, 7, n2p)
        wsend(block(g, 2, 0), g, 11, n2m)
        wsend(block(g, 2, 0), g, 23, partner)

    def s4(g, j):
        k = HOPS[j]
        wwait(block(g, k, 3), g, 4 + j)
        wsend(block(g, k, 3, 0, 32), g, 12 + j, n2p)
        wsend(block(g, k, 3), g, 24 + j, partner)
        wwait(block(g, k, 1), g, 8 + j)
        wsend(block(g, k, 1, 32, 32), g, 16 + j, n2m)
        wsend(block(g, k, 1), g, 28 + j, partner)

    def s5(g, j):
        k = HOPS[j]
        wwait(block(g, k, 2, 0, 32), g, 12 + j)
        wwait(block(g, k, 2, 32, 32), g, 16 + j)
        wsend(block(g, k, 2), g, 32 + j, partner)

    def s6(g):
        for j in range(4):
            for q, k2 in enumerate((0, 3, 1, 2)):
                wwait(other(g, HOPS[j], k2), g, 20 + 4 * q + j)

    def log_decay(h):
        ratio = (2 * x + h).astype(F32) * (1.0 / (HEADS - 1))
        return (float(np.log(0.05)) + ratio * float(np.log(18.0))) * (1.0 / SEQ)

    ld = [log_decay(0), log_decay(1)]
    ldc = log_decay(c)

    def power(e):
        return jnp.exp(jnp.full((1, 512), e, F32))

    def flag(cond):
        return jnp.where(cond, 1.0, 0.0).astype(F32)

    def loop(n, f):
        def step(i, carry):
            f(i)
            return carry

        lax.fori_loop(0, n, step, 0)

    def rows_of(i, n):
        return pl.ds(pl.multiple_of(i * n, n), n)

    def tables():
        cb, sb = coarsev[0:1, :], coarsev[1:2, :]

        def rot(i):
            r = rows_of(i, 128)
            cf, sf = finev[0, r, :], finev[1, r, :]
            ROT[0, r, :] = cf * cb - sf * sb
            ROT[1, r, :] = sf * cb + cf * sb

        loop(4, rot)

        def weight(i):
            r = rows_of(i, 64)
            t = lax.broadcasted_iota(jnp.int32, (64, 512), 0) + i * 64
            s = lax.broadcasted_iota(jnp.int32, (64, 512), 1)
            off = t - s
            offf = jnp.maximum(off, 0).astype(F32)
            for h in range(2):
                WT[h, r, :] = jnp.where(off >= 0, jnp.exp(ld[h] * offf), 0.0)

        loop(8, weight)

    def rotate(a, r):
        front, back = a[:, :128], a[:, 128:]
        cos, sin = ROT[0, r, :], ROT[1, r, :]
        return front * cos - back * sin, front * sin + back * cos

    def matmul(g, n):
        cols = pl.ds(pl.multiple_of(n * 256, 256), 256)
        w = W[g, :, :, :, :, cols].reshape(2048, 256)
        lhs = N[...].reshape(512, 2048)
        return jnp.dot(lhs, w, preferred_element_type=F32).astype(BF), cols

    def project(g, first, count):
        def step(i):
            res, cols = matmul(g, first + i)
            PV[g, :, cols] = res

        loop(count, step)

    def keys():
        for h in range(2):

            def step(i, h=h):
                r = rows_of(i, 128)
                front, back = rotate(PV[0, r, h * 256 : h * 256 + 256].astype(F32), r)
                RK[h, r, 0:128] = (front * 0.0625).astype(BF)
                RK[h, r, 128:256] = (back * 0.0625).astype(BF)

            loop(4, step)
            s = lax.broadcasted_iota(jnp.int32, (512, 1), 0).astype(F32)
            trailing = jnp.exp(ld[h] * (511.0 - s))
            weighted = (RK[h].astype(F32) * trailing).astype(BF)
            CF[h] = lax.dot_general(
                weighted,
                PV[0, :, 512 + h * 512 : 1024 + h * 512],
                (((0,), (0,)), ((), ())),
                preferred_element_type=F32,
            )
        PS[...] = CF[1 - c].astype(BF)
        send(PS, PC, sss.at[0], srs.at[0], partner)

    def state1():
        arrived(PC, sss.at[0], srs.at[0])
        d = power(ldc * 512.0)
        a = d * flag(c == 0) + flag(c == 1)
        b = d * flag(c == 1) + flag(c == 0)
        total = CF[c] * a + PC[...].astype(F32) * b
        TB[...] = total.astype(BF).reshape(4, 64, 512)
        TS[y] = TB[y]
        for k in (1, 3, 2):
            yy = (y + k) % 4
            send(TB.at[yy], TS.at[y], sss.at[k], srs.at[k], place(z, yy))

    def state2():
        for k in (1, 3, 2):
            arrived(TS.at[(y + 4 - k) % 4], sss.at[k], srs.at[k])
        total = TS[3].astype(F32)
        for yy in range(3):
            total += TS[yy].astype(F32) * power(ldc * (1024.0 * (3 - yy)))
        SZ[z] = total.astype(BF)
        for k in (1, 3, 2):
            send(SZ.at[z], SZ.at[z], sss.at[3 + k], srs.at[3 + k], place((z + k) % 4, y))

    def state3():
        for k in (1, 3, 2):
            arrived(SZ.at[(z + 4 - k) % 4], sss.at[3 + k], srs.at[3 + k])
        acc = jnp.zeros((64, 512), F32)
        for zz in range(3):
            e = jnp.maximum(z - 1 - zz, 0).astype(F32) * 4096.0
            acc += SZ[zz].astype(F32) * (power(ldc * e) * flag(zz < z))
        step = power(ldc * 1024.0)
        for yy in range(4):
            SB[yy] = acc.astype(BF)
            if yy < 3:
                acc = acc * step + TS[yy].astype(F32)
        SF[y] = SB[y]
        for k in (1, 3, 2):
            yy = (y + k) % 4
            send(SB.at[yy], SF.at[y], sss.at[6 + k], srs.at[6 + k], place(z, yy))

    def state4():
        for k in (1, 3, 2):
            arrived(SF.at[(y + 4 - k) % 4], sss.at[6 + k], srs.at[6 + k])
        d = power(ldc * 512.0)
        s = SF[...].reshape(256, 512).astype(F32)
        one, zero = flag(c == 1), flag(c == 0)
        STS[...] = (s * (d * zero + one) + CF[c] * zero).astype(BF)
        STM[c] = (s * (d * one + zero) + PC[...].astype(F32) * one).astype(BF)
        send(STS, STM.at[c], sss.at[10], srs.at[10], partner)

    def gate_input():
        def step(i):
            r = rows_of(i, 64)
            value = PV[1, r, 512:1024].astype(F32)
            switch = PV[1, r, 1024:1536].astype(F32)
            gated = (value / (1.0 + jnp.exp(-switch))).astype(BF).astype(F32)
            GP[pl.ds(pl.multiple_of(i * 64 + 32, 32), 64), :] = gated

        loop(8, step)
        HS[...] = GP[512:544, :].astype(BF)
        send(HS, HR, sss.at[11], srs.at[11], after)

    def scores():
        for h in range(2):

            def step(i, h=h):
                r = rows_of(i, 128)
                front, back = rotate(PV[1, r, h * 256 : h * 256 + 256].astype(F32), r)
                RQ[h, r, 0:128] = front.astype(BF)
                RQ[h, r, 128:256] = back.astype(BF)

            loop(4, step)

            def attend(i, h=h):
                r = rows_of(i, 256)
                sc = lax.dot_general(
                    RQ[h, r, :], RK[h], (((1,), (1,)), ((), ())), preferred_element_type=F32
                )
                sc = (sc * WT[h, r, :]).astype(BF)
                RAW[h, r, :] = jnp.dot(
                    sc, PV[0, :, 512 + h * 512 : 1024 + h * 512], preferred_element_type=F32
                )

            loop(2, attend)

    def convolve():
        arrived(HR, sss.at[11], srs.at[11])
        GP[0:32, :] = HR[...].astype(F32) * flag(sp > 0)

        def step(i):
            base = pl.multiple_of((i // 2) * 64, 64)
            cols = pl.ds(pl.multiple_of((i % 2) * 256, 256), 256)
            window = GP[pl.ds(base, 96), cols]
            acc = jnp.zeros((64, 256), F32)
            for q in range(8):
                shifted = window if q == 0 else pltpu.roll(window, 96 - q, axis=0)
                for k in range(5):
                    w = 8 * k + q - 2
                    if 0 <= w < KW:
                        acc += shifted[8 * k : 8 * k + 64] * tapv[w : w + 1, cols]
            CV[pl.ds(base, 64), cols] = acc

        loop(16, step)

        def norm(i):
            r = rows_of(i, 64)
            a = CV[r, :]
            a = a - jnp.mean(a, axis=-1, keepdims=True)
            spread = jnp.mean(a * a, axis=-1, keepdims=True)
            a = a * lax.rsqrt(spread + layer_eps) * lgainv[...] + lshiftv[...]
            CV[r, :] = silu(a)

        loop(8, norm)

    def finish():
        arrived(STM.at[1 - c], sss.at[10], srs.at[10])
        for h in range(2):

            def step(i, h=h):
                r = rows_of(i, 256)
                cross = jnp.dot(RQ[h, r, :], STM[h], preferred_element_type=F32)
                t = lax.broadcasted_iota(jnp.int32, (256, 1), 0) + i * 256
                raw = RAW[h, r, :] + cross * jnp.exp(ld[h] * (t + 1).astype(F32))
                raw = raw - jnp.mean(raw, axis=-1, keepdims=True)
                spread = jnp.mean(raw * raw, axis=-1, keepdims=True)
                RAW[h, r, :] = raw * lax.rsqrt(spread + group_eps)

            loop(2, step)

    def gates(h):
        def step(i):
            res, cols = matmul(2, h * 2 + i)
            g = silu(res.astype(F32))
            part = pl.ds(pl.multiple_of(i * 256, 256), 256)
            a = RAW[h, :, part] if h < 2 else CV[:, part]
            HID[:, cols] = (a * g).astype(BF)

        loop(2, step)

    def out_piece(zz):
        w = W[3, zz].reshape(512, 1536)
        for half in range(2):
            part = lax.dot_general(
                HID[...],
                w[half * 256 : half * 256 + 256],
                (((1,), (1,)), ((), ())),
                preferred_element_type=F32,
            )
            OP[zz, :, :, half * 256 : half * 256 + 256] = part.astype(BF).reshape(4, 128, 256)

    xl, xr, xf = (x + 3) % 4, (x + 1) % 4, (x + 2) % 4

    def reduce1(n):
        send(OP.at[n, xf, pl.ds(0, 64), :], RA.at[n, 0], rss.at[n, 0], rrs.at[n, 0], xp)
        send(OP.at[n, xf, pl.ds(64, 64), :], RA.at[n, 1], rss.at[n, 1], rrs.at[n, 1], xm)

    def reduce2(n):
        arrived(RA.at[n, 0], rss.at[n, 0], rrs.at[n, 0])
        OP[n, xr, 0:64, :] = (OP[n, xr, 0:64, :].astype(F32) + RA[n, 0].astype(F32)).astype(BF)
        send(OP.at[n, xr], RB.at[n, 0], rss.at[n, 2], rrs.at[n, 2], xp)
        arrived(RA.at[n, 1], rss.at[n, 1], rrs.at[n, 1])
        OP[n, xl, 64:128, :] = (OP[n, xl, 64:128, :].astype(F32) + RA[n, 1].astype(F32)).astype(BF)
        send(OP.at[n, xl], RB.at[n, 1], rss.at[n, 3], rrs.at[n, 3], xm)

    written = []

    def reduce3(n):
        arrived(RB.at[n, 0], rss.at[n, 2], rrs.at[n, 2])
        arrived(RB.at[n, 1], rss.at[n, 3], rrs.at[n, 3])
        total = OP[n, x].astype(F32) + RB[n, 0].astype(F32) + RB[n, 1].astype(F32)
        OUTV[n] = total.astype(BF)
        cp = pltpu.make_async_copy(OUTV.at[n], out.at[:, pl.ds(n * 512, 512)], osem.at[n])
        cp.start()
        written.append(cp)

    s1(0)
    loads[2].wait()
    loads[3].wait()

    def normalize(i):
        r = rows_of(i, 64)
        tk = tokv[r, :].astype(F32)
        scale = lax.rsqrt(jnp.mean(tk * tk, axis=-1, keepdims=True) + rms_eps)
        N[x, r, :] = (tk * scale * gainv[...]).astype(BF)

    loop(2, normalize)
    for cp in loads[4:]:
        cp.wait()
    s1(1)
    s2(0)
    send(N.at[x], N.at[x], nss.at[0], nrs.at[0], xp)
    send(N.at[x], N.at[x], nss.at[1], nrs.at[1], xm)

    def rows_on():
        arrived(N.at[xl], nss.at[0], nrs.at[0])
        left = N.at[xl, pl.ds(0, 64), :]
        send(left, left, nss.at[2], nrs.at[2], xp)
        arrived(N.at[xr], nss.at[1], nrs.at[1])
        right = N.at[xr, pl.ds(64, 64), :]
        send(right, right, nss.at[3], nrs.at[3], xm)

    def rows_in():
        arrived(N.at[xf, pl.ds(0, 64), :], nss.at[2], nrs.at[2])
        arrived(N.at[xf, pl.ds(64, 64), :], nss.at[3], nrs.at[3])

    tasks = {
        (0, 0): [rows_on, tables],
        (0, 5): [rows_in],
        (1, 0): [lambda: project(0, 0, 2)],
        (1, 1): [lambda: project(0, 2, 2)],
        (1, 2): [lambda: project(0, 4, 2)],
        (1, 3): [keys],
        (1, 4): [state1],
        (2, 0): [state2, lambda: project(1, 0, 2)],
        (2, 1): [lambda: project(1, 2, 2)],
        (2, 2): [lambda: project(1, 4, 2), gate_input],
        (2, 3): [state3],
        (2, 4): [scores],
        (2, 5): [state4],
        (3, 0): [convolve],
        (3, 1): [finish],
        (3, 2): [lambda: gates(0)],
        (3, 3): [lambda: gates(1)],
        (3, 4): [lambda: gates(2)],
    }

    def slot(g, k):
        for f in tasks.get((g, k), ()):
            f()

    for g in range(4):
        s3(g)
        if g + 2 < 4:
            s1(g + 2)
        s3b(g)
        if g + 1 < 4:
            s2(g + 1)
        slot(g, 0)
        for j in range(4):
            s4(g, j)
            slot(g, 1 + j)
        for j in range(4):
            s5(g, j)
        slot(g, 5)
        s6(g)

    out_piece(0)
    reduce1(0)
    out_piece(1)
    reduce1(1)
    reduce2(0)
    out_piece(2)
    reduce1(2)
    reduce2(1)
    out_piece(3)
    reduce1(3)
    reduce2(2)
    reduce2(3)
    for n in range(4):
        reduce3(n)
    for cp in written:
        cp.wait()
    for cp in sends:
        cp.wait_send()


def layer(tokens, gain, wq, wk, wv, wrg, wuv, wug, wcg, taps, lgain, lshift, wro, wco):
    any_spec = pl.BlockSpec(memory_space=pl.ANY)
    fine, coarse = rotation_tables()
    vm = pltpu.VMEM
    dma = pltpu.SemaphoreType.DMA
    row = lambda a: a.reshape(1, -1)
    return pl.pallas_call(
        body,
        out_shape=jax.ShapeDtypeStruct((128, 2048), BF),
        in_specs=[any_spec] * 16,
        out_specs=any_spec,
        scratch_shapes=[
            vm((4, 4, 4, 2, 64, 1536), BF),
            vm((4, 128, 2048), BF),
            vm((128, 2048), BF),
            vm((1, 2048), F32),
            vm((KW, 512), F32),
            vm((1, 512), F32),
            vm((1, 512), F32),
            vm((2, 512, 128), F32),
            vm((2, 128), F32),
            vm((2, 512, 1536), BF),
            vm((2, 512, 128), F32),
            vm((2, 512, 512), F32),
            vm((2, 512, 256), BF),
            vm((2, 512, 256), BF),
            vm((2, 256, 512), F32),
            vm((256, 512), BF),
            vm((256, 512), BF),
            vm((4, 64, 512), BF),
            vm((4, 64, 512), BF),
            vm((4, 64, 512), BF),
            vm((4, 64, 512), BF),
            vm((4, 64, 512), BF),
            vm((256, 512), BF),
            vm((2, 256, 512), BF),
            vm((2, 512, 512), F32),
            vm((544, 512), F32),
            vm((32, 512), BF),
            vm((32, 512), BF),
            vm((512, 512), F32),
            vm((512, 1536), BF),
            vm((4, 4, 128, 512), BF),
            vm((4, 2, 64, 512), BF),
            vm((4, 2, 128, 512), BF),
            vm((4, 128, 512), BF),
            dma((16,)),
            dma((4, 36)),
            dma((4, 36)),
            dma((4,)),
            dma((4,)),
            dma((12,)),
            dma((12,)),
            dma((4, 4)),
            dma((4, 4)),
            dma((4,)),
        ],
        compiler_params=pltpu.CompilerParams(
            collective_id=0, has_side_effects=True, vmem_limit_bytes=60 * 1024 * 1024
        ),
        name="layer",
    )(
        tokens, row(gain), wq, wk, wv, wrg, wuv, wug, wcg, wro, wco,
        taps, row(lgain), row(lshift), jnp.asarray(fine), jnp.asarray(coarse),
    )


def solution(mesh):
    weight = P("sp", "tp")
    rows = P(("sp", "tp"), None)
    return jax.shard_map(
        layer,
        mesh=mesh,
        in_specs=(rows, P()) + (weight,) * 7 + (P(),) * 3 + (weight,) * 2,
        out_specs=rows,
        check_vma=False,
    )
```

time: 282 us -> 118 us (0.42)
  waiting for transfers between devices: 101 us -> 0 us
  Pallas kernels: 92 us -> 115 us
  other arithmetic: 21.3 us -> 0 us
  blocking collectives: 21 us -> 0 us
  matrix products: 18.9 us -> 0 us
  between operations: 13.4 us -> 0.01 us
  local copies, waits for them, and re-layouts: 11.4 us -> 1.88 us
    all_gather x3 -> x0, waiting for transfers between devices: 70.7 us -> none  [entering(): pieces = jax.tree.map(lambda part: lax.all_gather(part, axis), total)]
    reduce_scatter x1 -> x0, waiting for transfers between devices: 30 us -> none  [local_b(): lax.psum_scatter(contract(jnp.concatenate([retain_hidden, convolve_hidden...]
    pallas_call x1, Pallas kernels: 92 us -> 115 us  [layer(): pl.pallas_call(body, out_shape=jax.ShapeDtypeStruct((128, 2048), BF), in_...]
    all_gather x3 -> x0, blocking collectives: 21 us -> none  [entering(): pieces = jax.tree.map(lambda part: lax.all_gather(part, axis), total)]
    dot_general x4 -> x0, matrix products: 18.9 us -> none  [the longest x1 7.54 us: contract(): lax.dot_general(hidden, matrix, (((1,), (1,)), ((), ())), preferred_eleme...]
    add x3 -> x0, other arithmetic: 6.66 us -> none  [the longest x2 6.66 us: join_states(): later[0][:, None, None] * earlier[1] + later[1]]
    slice x6 -> x0, local copies, waits for them, and re-layouts: 6.39 us -> none  [the longest x2 2.36 us: convolve_branch(): tap_slice[tap_index]]
    reduce_sum x3 -> x0, other arithmetic: 5.17 us -> none  [the longest x1 4.65 us: convolve_branch(): average = jnp.mean(grouped, axis=-1, keepdims=True)]
  transfers between devices with their start and end apart: 5 -> 0, of which waited for: 4 -> 0; matrix products, arithmetic and copies ran while one was open for 6% -> 0% of each run, Pallas kernels for 0% -> 0%
where the time goes in v2:
time: 118 us; the launch traced here: 117 us
  Pallas kernels  115 us (97%)
  local copies, waits for them, and re-layouts  1.88 us (2%)
    pallas_call x1, Pallas kernels, layer(): pl.pallas_call(body, out_shape=jax.ShapeDtypeStruct((128, 2048), BF), in_...  115 us

profile of v2, /device:TPU:0, one launch (start us, length us, event | category | flops | bytes accessed | tf_op | source)
XLA Modules:
  0.0 117.2 jit_solution(12914456345662025979)
XLA Ops:
  0.0 115.3 %layer.1 = bf16[128,2048]{1,0:T(8,128)(2,1)} custom-call(bf16[128,2048]{1,0:T(8,128)(2,1)} %tok.1, f32[1,2048]{1,0:T(1,128)} %bitcast.3, bf16[64,512]{1,0:T(8,128)(2,1)} %wq.1, bf16[64,512]{1,0:T(8,128)(2,1)} %wk.1, bf16[64,1024]{1,0:T(8,128)(2,1)} %wv.1, bf16[64,1024]{1,0:T(8,128)(2,1)} %wrg.1, bf16[64,512]{1,0:T(8,128)(2,1)} %wuv.1, bf16[64,512]{1,0:T(8,128)(2,1)} %wug.1, ...), custom_call_target="tpu_custom_call" | custom-call | tf_op jit(solution)/shard_map/layer/pallas_call | solution.py:585
  115.3 1.9 %copy.18 = bf16[128,2048]{1,0:T(8,128)(2,1)} copy(bf16[128,2048]{1,0:T(8,128)(2,1)} %layer.1) | data formatting | bytes 1048576
